TPU v7x, 32 devices: a whole 2x2x4 slice. The times are simulated.
32 devices in a mesh: grp: 2 (over y), sp: 8 (over z, core), tp: 2 (over x).
Axes of the slice: x: 2, y: 2, z: 4, core: 2. Of those that a mesh axis runs over, the one named last changes fastest.
Arguments:
- query_plain: bfloat16 [2560, 1024], P(('grp', 'sp'), 'tp'), parts along dimension 0, may hold values from -6 to 6
- query_turn: bfloat16 [2560, 512], P(('grp', 'sp'), 'tp'), parts along dimension 0, may hold values from -40 to 40, as said below
- latent: bfloat16 [2560, 512], P(('grp', 'sp')), parts along dimension 0, may hold values from -6 to 6
- key_turn: bfloat16 [2560, 64], P(('grp', 'sp')), parts along dimension 0, may hold values from -40 to 40, as said below
- latent_norm_scale: bfloat16 [512], replicated, may hold values from 0.099609375 to 1.8984375
- plain_key_matrix: bfloat16 [512, 1024], P(None, 'tp'), may hold values from -0.25 to 0.25
- value_matrix: bfloat16 [512, 1024], P(None, 'tp'), may hold values from -0.25 to 0.25
- residual: bfloat16 [2560, 2048], P(('grp', 'sp', 'tp')), parts along dimension 0, may hold values from -6 to 6
- out_weight: bfloat16 [1024, 2048], replicated, may hold values from -6 to 6
- ffn_gain: bfloat16 [2048], replicated, may hold values from 0.099609375 to 1.8984375
- gate_weight: bfloat16 [8, 2048, 1024], P('sp', None, 'tp'), may hold values from -1 to 1
- up_weight: bfloat16 [8, 2048, 1024], P('sp', None, 'tp'), may hold values from -1 to 1
- down_weight: bfloat16 [8, 1024, 2048], P('sp', 'tp'), may hold values from -0.0625 to 0.0625
- routes: int32 [2560, 4], P(('grp', 'sp', 'tp')), parts along dimension 0, may hold values from 0 to 7, all different within a row; in each aligned block of 80 rows (0 to 79, 80 to 159, ...) at most 60 rows name the same one
- route_weights: float32 [2560, 4], P(('grp', 'sp', 'tp')), parts along dimension 0, may hold values from 0.1 to 0.6
Outputs:
- mixed: bfloat16 [2560, 2048], P(('grp', 'sp', 'tp')), parts along dimension 0
There are 2 independent parts, one for each index of `grp`. A program takes and returns all parts, laid end to end along the dimension named above; an argument that names none is the same for every part. Nothing has to cross between parts.
Inputs may be any that keep to these rules, and one draw needn't show every extreme that they name: `query_turn`: in the hidden draw some rows are large. `key_turn`: in the hidden draw some rows are large. `routes`: each row names 4 different experts. In each aligned block of 80 rows (the rows of one device) no expert is named more than 60 times, a bound that some block reaches.
All inputs are finite; a program needn't handle non-finite values.
Results may differ from a plain program's by a relative error of at most 0.015.
Values may be sent and summed in bfloat16 or wider, within the bound.
A program may use at most 128 MiB of HBM per device.

v0:
```python
import jax
import jax.numpy as jnp
from jax import lax
from jax.sharding import PartitionSpec as P

PLAIN_HEAD_WIDTH = 128
QK_ROPE = 64
VALUE_WIDTH = 128
GRID_W = 64


theta = 10000.0
eps = 1e-06
limit = 7.0
slope = 1.702


def turn(vector, row_shift, col_shift):
    width = vector.shape[-1]
    count = width // 4
    half = width // 2
    freqs = theta ** (-jnp.arange(count, dtype=jnp.float32) / count)
    extra = (1,) * (vector.ndim - 2)
    pieces = []
    for portion, shift in ((vector[..., :half], row_shift), (vector[..., half:], col_shift)):
        angle = (shift.astype(jnp.float32)[:, None] * freqs[None, :]).reshape(
            (shift.shape[0],) + extra + (count,)
        )
        lower = portion[..., :count]
        upper = portion[..., count:]
        pieces.append(
            jnp.concatenate(
                [
                    lower * jnp.cos(angle) - upper * jnp.sin(angle),
                    lower * jnp.sin(angle) + upper * jnp.cos(angle),
                ],
                axis=-1,
            )
        )
    return jnp.concatenate(pieces, axis=-1)


def norm_scale(values, gain):
    wide = values.astype(jnp.float32)
    return (
        wide
        * lax.rsqrt(jnp.mean(wide * wide, axis=-1, keepdims=True) + eps)
        * gain.astype(jnp.float32)
    )


def expert_active(rows, gate_w, up_w):
    gate_pre = jnp.minimum(jnp.dot(rows, gate_w, preferred_element_type=jnp.float32), limit)
    up_pre = jnp.clip(jnp.dot(rows, up_w, preferred_element_type=jnp.float32), -limit, limit)
    return ((up_pre + 1.0) * gate_pre * jax.nn.sigmoid(slope * gate_pre)).astype(jnp.bfloat16)


def expert_whole(rows, gate_w, up_w, down_w, groups):
    active = expert_active(rows, gate_w, up_w)
    piece = down_w.shape[0] // groups
    total = jnp.zeros((rows.shape[0], down_w.shape[1]), jnp.float32)
    for index in range(groups):
        product = jnp.dot(
            active[:, index * piece : (index + 1) * piece],
            down_w[index * piece : (index + 1) * piece],
            preferred_element_type=jnp.float32,
        )
        total = total + product.astype(jnp.bfloat16).astype(jnp.float32)
    return total.astype(jnp.bfloat16)


def on_device(
    query_plain,
    query_turn,
    latent,
    key_turn,
    latent_norm_scale,
    plain_key_matrix,
    value_matrix,
    residual,
    out_weight,
    ffn_gain,
    gate_weight,
    up_weight,
    down_weight,
    routes,
    route_weights,
):
    tok_dev = latent.shape[0]
    heads_dev = query_plain.shape[1] // PLAIN_HEAD_WIDTH
    model_width = residual.shape[1]
    place = lax.axis_index("sp") * tok_dev + jnp.arange(tok_dev, dtype=jnp.int32)
    grid_row = place // GRID_W
    grid_col = place % GRID_W
    normed_latent = norm_scale(latent, latent_norm_scale).astype(jnp.bfloat16)
    key_plain = jnp.dot(normed_latent, plain_key_matrix, preferred_element_type=jnp.float32).astype(
        jnp.bfloat16
    )
    values = jnp.dot(normed_latent, value_matrix, preferred_element_type=jnp.float32).astype(
        jnp.bfloat16
    )
    key_rot = turn(key_turn.astype(jnp.float32), grid_row, grid_col).astype(jnp.bfloat16)
    key_pairs = key_rot.reshape(tok_dev // 2, 2 * QK_ROPE)
    query_rot = turn(
        query_turn.astype(jnp.float32).reshape(tok_dev, heads_dev, QK_ROPE), grid_row, grid_col
    ).astype(jnp.bfloat16)
    plain_query = query_plain.reshape(tok_dev, heads_dev, PLAIN_HEAD_WIDTH)
    scale = (PLAIN_HEAD_WIDTH + QK_ROPE) ** (-0.5)
    most = jnp.full((heads_dev, tok_dev), -jnp.inf, jnp.float32)
    total = jnp.zeros((heads_dev, tok_dev), jnp.float32)
    summed = jnp.zeros((heads_dev, tok_dev, VALUE_WIDTH), jnp.float32)
    piece_keys = lax.all_gather(key_plain, "sp", axis=0, tiled=True)
    piece_values = lax.all_gather(values, "sp", axis=0, tiled=True)
    piece_pairs = lax.all_gather(key_pairs, "sp", axis=0, tiled=True)
    count = piece_keys.shape[0]
    piece_rot = piece_pairs.reshape(count, QK_ROPE)
    new_most = []
    new_total = []
    new_summed = []
    for head in range(heads_dev):
        head_keys = piece_keys[:, head * PLAIN_HEAD_WIDTH : (head + 1) * PLAIN_HEAD_WIDTH]
        head_values = piece_values[:, head * VALUE_WIDTH : (head + 1) * VALUE_WIDTH]
        scores = (
            jnp.einsum(
                "qd,kd->qk", plain_query[:, head], head_keys, preferred_element_type=jnp.float32
            )
            + jnp.einsum(
                "qd,kd->qk", query_rot[:, head], piece_rot, preferred_element_type=jnp.float32
            )
        ) * scale
        peak = jnp.max(scores, axis=1)
        factor = jnp.exp(most[head] - peak)
        weights = jnp.exp(scores - peak[:, None])
        new_total.append(total[head] * factor + jnp.sum(weights, axis=1))
        new_summed.append(
            summed[head] * factor[:, None]
            + jnp.dot(weights.astype(jnp.bfloat16), head_values, preferred_element_type=jnp.float32)
        )
        new_most.append(peak)
    total = jnp.stack(new_total)
    summed = jnp.stack(new_summed)
    attended = jnp.transpose((summed / total[..., None]).astype(jnp.bfloat16), (1, 0, 2)).reshape(
        tok_dev, heads_dev * VALUE_WIDTH
    )
    rows_dev = residual.shape[0]
    own_rows = lax.dynamic_slice_in_dim(
        out_weight, lax.axis_index("tp") * heads_dev * VALUE_WIDTH, heads_dev * VALUE_WIDTH, 0
    )
    projected = lax.psum_scatter(
        jnp.dot(attended, own_rows, preferred_element_type=jnp.float32).astype(jnp.bfloat16),
        "tp",
        scatter_dimension=0,
        tiled=True,
    ).astype(jnp.float32)
    hidden = (residual.astype(jnp.float32) + projected).astype(jnp.bfloat16)
    normed = norm_scale(hidden, ffn_gain).astype(jnp.bfloat16)
    top_count = routes.shape[1]
    experts_all = lax.axis_size("sp") * gate_weight.shape[0]
    capacity = min(rows_dev, max(2, rows_dev * top_count * 3 // (2 * experts_all)))
    flat_routes = routes.reshape(rows_dev * top_count)
    marks = (flat_routes[:, None] == jnp.arange(experts_all, dtype=jnp.int32)[None, :]).astype(
        jnp.int32
    )
    earlier = jnp.cumsum(marks, axis=0, dtype=jnp.int32) - marks
    slots = jnp.sum(earlier * marks, axis=1, dtype=jnp.int32)
    target = flat_routes * capacity + slots
    chosen = (
        target.reshape(rows_dev, top_count)[None, :, :]
        == jnp.arange(experts_all * capacity, dtype=jnp.int32)[:, None, None]
    )
    dispatch_table = jnp.sum(chosen.astype(jnp.bfloat16), axis=2)
    outgoing = jnp.dot(dispatch_table, normed, preferred_element_type=jnp.float32).astype(
        jnp.bfloat16
    )
    outgoing = outgoing.reshape(experts_all, capacity, model_width)
    gate_w = gate_weight[0]
    up_w = up_weight[0]
    down_w = down_weight[0]
    group = lax.axis_size("tp")
    gate_full, up_full, down_full = (
        lax.all_gather(gate_w, "tp", axis=1, tiled=True),
        lax.all_gather(up_w, "tp", axis=1, tiled=True),
        lax.all_gather(down_w, "tp", axis=0, tiled=True),
    )
    arrived = lax.all_to_all(outgoing, "sp", split_axis=0, concat_axis=0, tiled=True)
    result_rows = expert_whole(
        arrived.reshape(experts_all * capacity, model_width), gate_full, up_full, down_full, group
    )
    returned = lax.all_to_all(
        result_rows.reshape(experts_all, capacity, model_width),
        "sp",
        split_axis=0,
        concat_axis=0,
        tiled=True,
    )
    picked = returned.reshape(experts_all * capacity, model_width)[target]
    picked = picked.reshape(rows_dev, top_count, model_width).astype(jnp.float32)
    return (hidden.astype(jnp.float32) + jnp.sum(route_weights[..., None] * picked, axis=1)).astype(
        jnp.bfloat16
    )


def solution(mesh):
    placed = (
        P(("grp", "sp"), "tp"),
        P(("grp", "sp"), "tp"),
        P(("grp", "sp"), None),
        P(("grp", "sp"), None),
        P(),
        P(None, "tp"),
        P(None, "tp"),
        P(("grp", "sp", "tp"), None),
        P(),
        P(),
        P("sp", None, "tp"),
        P("sp", None, "tp"),
        P("sp", "tp", None),
        P(("grp", "sp", "tp"), None),
        P(("grp", "sp", "tp"), None),
    )
    return jax.shard_map(
        on_device,
        mesh=mesh,
        in_specs=placed,
        out_specs=P(("grp", "sp", "tp"), None),
        check_vma=False,
    )
```

profile of v0, /device:TPU:9, one launch (start us, length us, event | category | flops | bytes accessed | tf_op | source)
XLA Modules:
  0.0 331.1 jit_solution(11522728959038800007)
XLA Ops:
  6.6 1.1 fusion.38
  7.7 0.7 convert_element_type.119
  8.4 1.9 convolution_convert_fusion.5
  10.3 2.1 convolution_convert_fusion.4
  12.7 0.2 multiply_cosine_fusion.1
  12.9 0.1 copy.35
  13.0 0.1 convert_element_type.125
  13.1 15.0 %all_gather.19 = bf16[640,128]{1,0:T(8,128)(2,1)S(1)} all-gather(bf16[80,128]{1,0:T(8,128)(2,1)S(1)} %convert_element_type.125), channel_id=1, replica_groups=mesh['grp'=2,'sp'=8,'tp'=2] {'sp'}, dimensions={0}, use_global_device_ids=true | all-gather | bytes 184320 | tf_op jit(solution)/shard_map/all_gather | solution.py:114
  28.1 0.2 reshape.367
  28.3 0.2 fusion.79
  28.7 7.1 %all-gather.9.cloned.1.call-done = bf16[1280,512]{1,0:T(8,128)(2,1)} async-done(((bf16[160,512]{1,0:T(8,128)(2,1)}), bf16[1280,512]{1,0:T(8,128)(2,1)}) %all-gather.9.cloned.1.call-update) | async-done | bytes 1310736 | tf_op jit(solution)/shard_map/all_gather | solution.py:112
  35.8 1.3 convolution_bitcast_fusion.3
  37.1 0.4 fusion.83
  37.5 0.3 convolution_bitcast_fusion.2
  37.8 0.4 fusion.82
  38.2 0.3 convolution_bitcast_fusion.1
  38.5 0.3 fusion.15
  38.8 0.3 fusion.17
  39.0 0.4 fusion.81
  39.4 0.3 fusion.19
  39.7 0.3 convolution_bitcast_fusion
  40.0 0.4 fusion.80
  40.4 0.9 copy-done.1
  41.3 0.3 fusion.21
  41.7 18.4 %all-gather.11.cloned.1.call-done = bf16[1280,512]{1,0:T(8,128)(2,1)} async-done(((bf16[160,512]{1,0:T(8,128)(2,1)}), bf16[1280,512]{1,0:T(8,128)(2,1)}) %all-gather.11.cloned.1.call-update) | async-done | bytes 1310736 | tf_op jit(solution)/shard_map/all_gather | solution.py:113
  60.1 1.4 fusion.14
  61.6 1.3 fusion.13
  62.9 0.3 fusion.12
  63.2 0.3 fusion.11
  63.6 3.0 convolution_convert_fusion.3
  66.7 0.5 all-gather.15.cloned.1.call-update
  67.3 0.5 all-gather.13.cloned.1.call-update
  67.8 0.1 copy.38
  67.9 0.1 eq.37
  68.0 0.9 reduce-window.6
  68.9 0.2 slice_reduce_fusion
  69.3 0.1 reduce_sum.94
  69.5 0.1 fusion.41
  69.6 12.7 %reduce-scatter.2.cloned.1.call-done = bf16[80,2048]{1,0:T(8,128)(2,1)} async-done(((bf16[160,2048]{1,0:T(8,128)(2,1)}), bf16[80,2048]{1,0:T(8,128)(2,1)}) %reduce-scatter.2.cloned.1.call-update) | async-done | bytes 327696 | tf_op jit(solution)/shard_map/reduce_scatter | solution.py:149
  82.4 1.2 fusion.23
  83.6 1.7 convolution_convert_fusion.2
  85.3 1.6 reshape.371
  86.8 5.6 %all-to-all-start = ((bf16[8,60,2048]{2,1,0:T(8,128)(2,1)}), bf16[8,60,2048]{2,1,0:T(8,128)(2,1)S(1)}, u32[]{:S(2)}, u32[]{:S(2)}) async-start(bf16[8,60,2048]{2,1,0:T(8,128)(2,1)} %reshape.371), calls=%async_computation.1 | async-start | bytes 4194304 | tf_op jit(solution)/shard_map/all_to_all | solution.py:185
  92.4 0.6 all-gather.17.cloned.1.call-update
  93.0 45.0 %all-to-all-done = bf16[8,60,2048]{2,1,0:T(8,128)(2,1)S(1)} async-done(((bf16[8,60,2048]{2,1,0:T(8,128)(2,1)}), bf16[8,60,2048]{2,1,0:T(8,128)(2,1)S(1)}, u32[]{:S(2)}, u32[]{:S(2)}) %all-to-all-start) | async-done | bytes 1966112 | tf_op jit(solution)/shard_map/all_to_all | solution.py:185
  138.0 1.5 reshape.372
  139.4 1.1 all-gather.15.cloned.1.call-done
  140.5 6.3 %fusion = f32[480,1024]{1,0:T(8,128)} fusion(bf16[480,2048]{1,0:T(8,128)(2,1)} %reshape.372, bf16[1,2048,1024]{2,1,0:T(8,128)(2,1)} %all-gather.15.cloned.1.call-done), kind=kOutput, calls=%fused_computation.1 | convolution fusion | flops 2013265920 | bytes 8126464 | tf_op jit(solution)/shard_map/dot_general | solution.py:53
  146.8 51.8 %all-gather.13.cloned.1.call-done = bf16[1,2048,1024]{2,1,0:T(8,128)(2,1)} async-done(((bf16[1,2048,512]{2,1,0:T(8,128)(2,1)}), bf16[1,2048,1024]{2,1,0:T(8,128)(2,1)}) %all-gather.13.cloned.1.call-update) | async-done | bytes 4194320 | tf_op jit(solution)/shard_map/all_gather | solution.py:182
  198.7 6.5 %multiply_convert_fusion = bf16[480,1024]{1,0:T(8,128)(2,1)} fusion(f32[480,1024]{1,0:T(8,128)} %fusion, bf16[480,2048]{1,0:T(8,128)(2,1)S(1)} %copy-done.5, bf16[1,2048,1024]{2,1,0:T(8,128)(2,1)} %all-gather.13.cloned.1.call-done), kind=kOutput, calls=%fused_computation.26 | convolution fusion | flops 2018181120 | bytes 9109504 | tf_op jit(solution)/shard_map/dot_general | solution.py:54
  205.1 51.7 %all-gather.17.cloned.1.call-done = bf16[1,1024,2048]{2,1,0:T(8,128)(2,1)} async-done(((bf16[1,512,2048]{2,1,0:T(8,128)(2,1)}), bf16[1,1024,2048]{2,1,0:T(8,128)(2,1)}) %all-gather.17.cloned.1.call-update) | async-done | bytes 4194320 | tf_op jit(solution)/shard_map/all_gather | solution.py:183
  256.8 3.1 convolution_convert_fusion
  259.9 0.1 copy-done.15
  260.1 1.2 add_convert_fusion
  261.3 1.5 reshape.373
  262.8 5.7 %all-to-all-start.1 = ((bf16[8,60,2048]{2,1,0:T(8,128)(2,1)}), bf16[8,60,2048]{2,1,0:T(8,128)(2,1)}, u32[]{:S(2)}, u32[]{:S(2)}) async-start(bf16[8,60,2048]{2,1,0:T(8,128)(2,1)} %reshape.373), calls=%async_computation.2 | async-start | bytes 4194304 | tf_op jit(solution)/shard_map/all_to_all | solution.py:189
  268.5 0.1 mul.305
  268.6 0.1 copy.37
  268.7 45.3 %all-to-all-done.1 = bf16[8,60,2048]{2,1,0:T(8,128)(2,1)} async-done(((bf16[8,60,2048]{2,1,0:T(8,128)(2,1)}), bf16[8,60,2048]{2,1,0:T(8,128)(2,1)}, u32[]{:S(2)}, u32[]{:S(2)}) %all-to-all-start.1) | async-done | bytes 1966112 | tf_op jit(solution)/shard_map/all_to_all | solution.py:189
  314.0 1.7 reshape.374
  315.8 3.0 gather_fusion
  318.8 2.6 reshape.378
  321.4 1.9 multiply_reduce_fusion
  323.4 0.8 fusion.26
  (65 shorter events, 0.9 us)
Async XLA Ops:
  6.5 1.9 copy-start
  6.5 6.0 %copy-start.10 = (bf16[160,64]{0,1:T(8,128)(2,1)S(1)}, bf16[160,64]{0,1:T(8,128)(2,1)}, u32[]{:S(2)}) copy-start(bf16[160,64]{0,1:T(8,128)(2,1)} %param.18) | copy-start | bytes 61444
  6.5 6.0 %copy-start.9 = (bf16[160,256]{1,0:T(8,128)(2,1)S(1)}, bf16[160,256]{1,0:T(8,128)(2,1)}, u32[]{:S(2)}) copy-start(bf16[160,256]{1,0:T(8,128)(2,1)} %param.16) | copy-start | bytes 245764
  6.5 21.7 %copy-start.8 = (bf16[160,512]{1,0:T(8,128)(2,1)S(1)}, bf16[160,512]{1,0:T(8,128)(2,1)}, u32[]{:S(2)}) copy-start(bf16[160,512]{1,0:T(8,128)(2,1)} %param.15) | copy-start | bytes 491524
  6.5 29.2 %all-gather.9.cloned.1.call-start = ((), (), s32[]{:S(2)}) async-start(), calls=%async_computation.3 | async-start | bytes 1474560 | tf_op jit(solution)/shard_map/all_gather | solution.py:112
  10.3 49.8 %all-gather.11.cloned.1.call-start = ((), (), s32[]{:S(2)}) async-start(), calls=%async_computation.4 | async-start | bytes 1474560 | tf_op jit(solution)/shard_map/all_gather | solution.py:113
  12.4 69.9 %reduce-scatter.2.cloned.1.call-start = ((), (), s32[]{:S(2)}) async-start(), calls=%async_computation.5 | async-start | bytes 983040 | tf_op jit(solution)/shard_map/reduce_scatter | solution.py:149
  35.8 1.8 copy-start.6
  40.4 0.9 copy-start.1
  60.1 2.8 copy-start.7
  60.1 3.1 copy-start.2
  66.6 1.2 copy-start.12
  66.6 2.9 copy-start.11
  66.6 15.7 %copy-start.3 = (bf16[80,2048]{1,0:T(8,128)(2,1)S(1)}, bf16[80,2048]{1,0:T(8,128)(2,1)}, u32[]{:S(2)}) copy-start(bf16[80,2048]{1,0:T(8,128)(2,1)} %param.22) | copy-start | bytes 983044
  66.6 73.9 %all-gather.15.cloned.1.call-start = ((), (), s32[]{:S(2)}) async-start(), calls=%async_computation.7 | async-start | bytes 6291456 | tf_op jit(solution)/shard_map/all_gather | solution.py:181
  67.2 131.4 %all-gather.13.cloned.1.call-start = ((), (), s32[]{:S(2)}) async-start(), calls=%async_computation.6 | async-start | bytes 6291456 | tf_op jit(solution)/shard_map/all_gather | solution.py:182
  86.8 51.1 %all-to-all-start = ((bf16[8,60,2048]{2,1,0:T(8,128)(2,1)}), bf16[8,60,2048]{2,1,0:T(8,128)(2,1)S(1)}, u32[]{:S(2)}, u32[]{:S(2)}) async-start(bf16[8,60,2048]{2,1,0:T(8,128)(2,1)} %reshape.371), calls=%async_computation.1 | async-start | bytes 4194304 | tf_op jit(solution)/shard_map/all_to_all | solution.py:185
  92.4 164.4 %all-gather.17.cloned.1.call-start = ((), (), s32[]{:S(2)}) async-start(), calls=%async_computation.8 | async-start | bytes 6291456 | tf_op jit(solution)/shard_map/all_gather | solution.py:183
  139.4 59.2 %copy-start.5 = (bf16[480,2048]{1,0:T(8,128)(2,1)S(1)}, bf16[480,2048]{1,0:T(8,128)(2,1)}, u32[]{:S(2)}) copy-start(bf16[480,2048]{1,0:T(8,128)(2,1)} %reshape.372) | copy-start | bytes 5898244
  256.8 3.1 copy-start.14
  256.8 3.2 copy-start.15
  262.8 5.8 %copy-start.13 = (f32[80,4]{0,1:T(4,128)S(1)}, f32[80,4]{0,1:T(4,128)}, u32[]{:S(2)}) copy-start(f32[80,4]{0,1:T(4,128)} %param.29) | copy-start | bytes 3844
  262.8 51.3 %all-to-all-start.1 = ((bf16[8,60,2048]{2,1,0:T(8,128)(2,1)}), bf16[8,60,2048]{2,1,0:T(8,128)(2,1)}, u32[]{:S(2)}, u32[]{:S(2)}) async-start(bf16[8,60,2048]{2,1,0:T(8,128)(2,1)} %reshape.373), calls=%async_computation.2 | async-start | bytes 4194304 | tf_op jit(solution)/shard_map/all_to_all | solution.py:189
  321.4 1.9 copy-start.4
Sparse Core Ops, SparseCore 0:
  10.4 25.3 all-gather.8
  37.4 22.6 all-gather.10
  66.7 15.5 reduce-scatter.1
  83.8 56.7 all-gather.14
  141.9 56.7 all-gather.12
  200.1 56.7 all-gather.16
where the time goes:
time: 336 us; the launch traced here: 331 us
  waiting for transfers between devices  235 us (70%)
  matrix products  32.9 us (10%)
  blocking collectives  15 us (4%)
  local copies, waits for them, and re-layouts  14.6 us (4%)
  between operations  13.9 us (4%)
  starting transfers between devices  11.5 us (3%)
  other arithmetic  8.38 us (2%)
    all_gather x1, waiting for transfers between devices, on_device(): lax.all_gather(up_w, 'tp', axis=1, tiled=True)  51.8 us
    all_gather x1, waiting for transfers between devices, on_device(): lax.all_gather(down_w, 'tp', axis=0, tiled=True)  51.7 us
    all_to_all x1, waiting for transfers between devices, on_device(): lax.all_to_all(result_rows.reshape(experts_all, capacity, model_width), '...  45.3 us
    all_to_all x1, waiting for transfers between devices, on_device(): lax.all_to_all(outgoing, 'sp', split_axis=0, concat_axis=0, tiled=True)  45 us
    all_gather x1, waiting for transfers between devices, on_device(): piece_values = lax.all_gather(values, 'sp', axis=0, tiled=True)  18.4 us
    all_gather x1, blocking collectives, on_device(): piece_pairs = lax.all_gather(key_pairs, 'sp', axis=0, tiled=True)  15 us
    reduce_scatter x1, waiting for transfers between devices, on_device(): lax.psum_scatter(jnp.dot(attended, own_rows, preferred_element_type=jnp.f...  12.7 us
    all_gather x1, waiting for transfers between devices, on_device(): piece_keys = lax.all_gather(key_plain, 'sp', axis=0, tiled=True)  7.11 us
  transfers between devices with their start and end apart: 8, of which 8 were waited for; matrix products, arithmetic and copies ran while one was open for 9% of the time, Pallas kernels for 0%

commit v1 on v0

v1 whole, which is shorter than its diff:
```python
import jax
import jax.numpy as jnp
from jax import lax
from jax.sharding import PartitionSpec as P

PLAIN_HEAD_WIDTH = 128
QK_ROPE = 64
VALUE_WIDTH = 128
GRID_W = 64


theta = 10000.0
eps = 1e-06
limit = 7.0
slope = 1.702


def turn(vector, row_shift, col_shift):
    width = vector.shape[-1]
    count = width // 4
    half = width // 2
    freqs = theta ** (-jnp.arange(count, dtype=jnp.float32) / count)
    extra = (1,) * (vector.ndim - 2)
    pieces = []
    for portion, shift in ((vector[..., :half], row_shift), (vector[..., half:], col_shift)):
        angle = (shift.astype(jnp.float32)[:, None] * freqs[None, :]).reshape(
            (shift.shape[0],) + extra + (count,)
        )
        lower = portion[..., :count]
        upper = portion[..., count:]
        pieces.append(
            jnp.concatenate(
                [
                    lower * jnp.cos(angle) - upper * jnp.sin(angle),
                    lower * jnp.sin(angle) + upper * jnp.cos(angle),
                ],
                axis=-1,
            )
        )
    return jnp.concatenate(pieces, axis=-1)


def norm_scale(values, gain):
    wide = values.astype(jnp.float32)
    return (
        wide
        * lax.rsqrt(jnp.mean(wide * wide, axis=-1, keepdims=True) + eps)
        * gain.astype(jnp.float32)
    )


def expert_active(rows, gate_w, up_w):
    gate_pre = jnp.minimum(jnp.dot(rows, gate_w, preferred_element_type=jnp.float32), limit)
    up_pre = jnp.clip(jnp.dot(rows, up_w, preferred_element_type=jnp.float32), -limit, limit)
    return ((up_pre + 1.0) * gate_pre * jax.nn.sigmoid(slope * gate_pre)).astype(jnp.bfloat16)


def on_device(
    query_plain,
    query_turn,
    latent,
    key_turn,
    latent_norm_scale,
    plain_key_matrix,
    value_matrix,
    residual,
    out_weight,
    ffn_gain,
    gate_weight,
    up_weight,
    down_weight,
    routes,
    route_weights,
):
    tok_dev = latent.shape[0]
    heads_dev = query_plain.shape[1] // PLAIN_HEAD_WIDTH
    model_width = residual.shape[1]
    place = lax.axis_index("sp") * tok_dev + jnp.arange(tok_dev, dtype=jnp.int32)
    grid_row = place // GRID_W
    grid_col = place % GRID_W
    normed_latent = norm_scale(latent, latent_norm_scale).astype(jnp.bfloat16)
    key_rot = turn(key_turn.astype(jnp.float32), grid_row, grid_col).astype(jnp.bfloat16)
    expert_ids = jnp.arange(lax.axis_size("sp"), dtype=jnp.int32)
    share = jnp.sum(
        route_weights[..., None] * (routes[..., None] == expert_ids).astype(jnp.float32), axis=1
    )
    latent_width = latent.shape[1]
    sent = jnp.concatenate([normed_latent, key_rot], axis=1)
    everyone = lax.all_gather(sent, "sp", axis=0, tiled=True)
    shares = lax.all_gather(share, ("sp", "tp"), axis=0, tiled=True)
    all_latent = everyone[:, :latent_width]
    all_rot = everyone[:, latent_width:]
    keys = jnp.dot(all_latent, plain_key_matrix, preferred_element_type=jnp.float32).astype(
        jnp.bfloat16
    )
    values = jnp.dot(all_latent, value_matrix, preferred_element_type=jnp.float32).astype(
        jnp.bfloat16
    )
    query_rot = turn(
        query_turn.astype(jnp.float32).reshape(tok_dev, heads_dev, QK_ROPE), grid_row, grid_col
    ).astype(jnp.bfloat16)
    scale = (PLAIN_HEAD_WIDTH + QK_ROPE) ** (-0.5)
    attended = []
    for head in range(heads_dev):
        span = slice(head * PLAIN_HEAD_WIDTH, (head + 1) * PLAIN_HEAD_WIDTH)
        scores = (
            jnp.einsum(
                "qd,kd->qk", query_plain[:, span], keys[:, span], preferred_element_type=jnp.float32
            )
            + jnp.einsum(
                "qd,kd->qk", query_rot[:, head], all_rot, preferred_element_type=jnp.float32
            )
        ) * scale
        weights = jnp.exp(scores - jnp.max(scores, axis=1, keepdims=True))
        summed = jnp.dot(
            weights.astype(jnp.bfloat16),
            values[:, head * VALUE_WIDTH : (head + 1) * VALUE_WIDTH],
            preferred_element_type=jnp.float32,
        )
        attended.append(
            (summed / jnp.sum(weights, axis=1, keepdims=True)).astype(jnp.bfloat16)
        )
    attended = jnp.concatenate(attended, axis=1)
    rows_dev = residual.shape[0]
    group = lax.axis_size("tp")
    swapped = lax.all_to_all(
        attended.reshape(group, rows_dev, heads_dev * VALUE_WIDTH),
        "tp",
        split_axis=0,
        concat_axis=0,
        tiled=True,
    )
    own_rows = jnp.transpose(swapped, (1, 0, 2)).reshape(rows_dev, group * heads_dev * VALUE_WIDTH)
    projected = jnp.dot(own_rows, out_weight, preferred_element_type=jnp.float32)
    hidden = (residual.astype(jnp.float32) + projected).astype(jnp.bfloat16)
    normed = norm_scale(hidden, ffn_gain).astype(jnp.bfloat16)
    rows = lax.all_gather(normed, ("sp", "tp"), axis=0, tiled=True)
    active = expert_active(rows, gate_weight[0], up_weight[0])
    product = jnp.dot(active, down_weight[0], preferred_element_type=jnp.float32)
    own_share = jnp.sum(
        jnp.where(expert_ids[None, :] == lax.axis_index("sp"), shares, 0.0), axis=1, keepdims=True
    )
    mixture = lax.psum_scatter(
        (own_share * product).astype(jnp.bfloat16),
        ("sp", "tp"),
        scatter_dimension=0,
        tiled=True,
    )
    return (hidden.astype(jnp.float32) + mixture.astype(jnp.float32)).astype(jnp.bfloat16)


def solution(mesh):
    placed = (
        P(("grp", "sp"), "tp"),
        P(("grp", "sp"), "tp"),
        P(("grp", "sp"), None),
        P(("grp", "sp"), None),
        P(),
        P(None, "tp"),
        P(None, "tp"),
        P(("grp", "sp", "tp"), None),
        P(),
        P(),
        P("sp", None, "tp"),
        P("sp", None, "tp"),
        P("sp", "tp", None),
        P(("grp", "sp", "tp"), None),
        P(("grp", "sp", "tp"), None),
    )
    return jax.shard_map(
        on_device,
        mesh=mesh,
        in_specs=placed,
        out_specs=P(("grp", "sp", "tp"), None),
        check_vma=False,
    )
```

time: 336 us -> 220 us (0.65)
  waiting for transfers between devices: 235 us -> 136 us
  local copies, waits for them, and re-layouts: 14.6 us -> 2.73 us
  blocking collectives: 15 us -> 23.9 us
  starting transfers between devices: 11.5 us -> 3.51 us
  matrix products: 32.9 us -> 28.3 us
    all_to_all x2 -> x1, waiting for transfers between devices: 90.3 us -> 3.83 us  [on_device(): lax.all_to_all(attended.reshape(group, rows_dev, heads_dev * VALUE_WIDTH)...]
    all_gather x5 -> x2, waiting for transfers between devices: 130 us -> 57.4 us  [the longest x1 31.4 us: on_device(): rows = lax.all_gather(normed, ('sp', 'tp'), axis=0, tiled=True)]
    reduce_scatter x1, waiting for transfers between devices: 12.7 us -> 74.7 us  [on_device(): lax.psum_scatter((own_share * product).astype(jnp.bfloat16), ('sp', 'tp')...]
    all_gather x1, blocking collectives: 15 us -> 23.9 us  [on_device(): shares = lax.all_gather(share, ('sp', 'tp'), axis=0, tiled=True)]
    all_to_all x2 -> x1, starting transfers between devices: 11.3 us -> 3.43 us  [on_device(): lax.all_to_all(attended.reshape(group, rows_dev, heads_dev * VALUE_WIDTH)...]
    reshape x6 -> x1, local copies, waits for them, and re-layouts: 6.48 us -> 0.01 us  [on_device(): jnp.transpose(swapped, (1, 0, 2))]
    dot_general x19 -> x16, matrix products: 26.6 us -> 20.7 us  [the longest x1 10.5 us: on_device(): jnp.dot(active, down_weight[0], preferred_element_type=jnp.float32)]
  transfers between devices with their start and end apart: 8 -> 4, of which waited for: 8 -> 4; matrix products, arithmetic and copies ran while one was open for 9% -> 1% of each run, Pallas kernels for 0% -> 0%
where the time goes in v1:
time: 220 us; the launch traced here: 216 us
  waiting for transfers between devices  136 us (62%)
  matrix products  28.3 us (13%)
  blocking collectives  23.9 us (11%)
  between operations  13.4 us (6%)
  other arithmetic  8.51 us (4%)
  starting transfers between devices  3.51 us (2%)
  local copies, waits for them, and re-layouts  2.73 us (1%)
    reduce_scatter x1, waiting for transfers between devices, on_device(): lax.psum_scatter((own_share * product).astype(jnp.bfloat16), ('sp', 'tp')...  74.7 us
    all_gather x1, waiting for transfers between devices, on_device(): rows = lax.all_gather(normed, ('sp', 'tp'), axis=0, tiled=True)  31.4 us
    all_gather x1, waiting for transfers between devices, on_device(): everyone = lax.all_gather(sent, 'sp', axis=0, tiled=True)  26.1 us
    all_gather x1, blocking collectives, on_device(): shares = lax.all_gather(share, ('sp', 'tp'), axis=0, tiled=True)  23.9 us
    dot_general x1, matrix products, on_device(): jnp.dot(active, down_weight[0], preferred_element_type=jnp.float32)  10.5 us
    dot_general x1, matrix products, expert_active(): jnp.dot(rows, gate_w, preferred_element_type=jnp.float32)  7.58 us
  transfers between devices with their start and end apart: 4, of which 4 were waited for; matrix products, arithmetic and copies ran while one was open for 1% of the time, Pallas kernels for 0%

profile of v1, /device:TPU:9, one launch (start us, length us, event | category | flops | bytes accessed | tf_op | source)
XLA Modules:
  0.0 216.3 jit_solution(17451108675109857187)
XLA Ops:
  6.5 0.0 copy-start
  6.5 0.0 all-gather.4.cloned.1.call-start
  6.6 1.2 fusion.37
  7.8 0.7 convert_element_type.92
  8.5 0.8 convert_element_type.94
  9.2 0.2 multiply_cosine_fusion
  9.5 0.1 copy.52
  9.6 0.1 copy.51
  9.7 0.1 copy.53
  9.8 0.1 copy.54
  9.9 1.0 fusion.39
  11.0 0.8 concatenate.13
  11.8 0.0 all-gather.4.cloned.1.call-update
  11.8 1.0 copy.55
  12.9 0.0 copy-start.3
  12.9 26.1 %all-gather.4.cloned.1.call-done = bf16[1280,576]{1,0:T(8,128)(2,1)} async-done(((bf16[160,576]{1,0:T(8,128)(2,1)}), bf16[1280,576]{1,0:T(8,128)(2,1)}) %all-gather.4.cloned.1.call-update) | async-done | bytes 1474576 | tf_op jit(solution)/shard_map/all_gather | solution.py:89
  39.0 0.0 copy-done.7
  39.0 2.2 convolution_convert_fusion.1
  41.1 0.0 copy-done.3
  41.1 0.0 copy-start.1
  41.2 0.3 convolution_bitcast_fusion
  41.4 0.3 convolution_bitcast_fusion.1
  41.7 0.3 convolution_bitcast_fusion.2
  42.0 0.0 copy-start.8
  42.0 0.3 convolution_bitcast_fusion.3
  42.3 0.3 copy-done.1
  42.6 0.4 fusion.63
  43.0 0.3 fusion.27
  43.3 0.0 copy-done.8
  43.3 0.8 convolution_convert_fusion
  44.1 0.3 fusion.18
  44.4 0.4 fusion.64
  44.8 0.3 fusion.25
  45.1 0.3 fusion.17
  45.5 0.4 fusion.66
  45.9 0.3 fusion.21
  46.1 0.3 fusion.15
  46.5 0.0 copy-start.4
  46.5 0.0 copy-start.2
  46.5 0.4 fusion.65
  46.9 0.3 fusion.23
  47.2 0.3 fusion.16
  47.5 0.7 pad_maximum_fusion
  48.2 3.4 %all-to-all-start = ((bf16[2,80,512]{2,1,0:T(8,128)(2,1)}), bf16[2,80,512]{2,1,0:T(8,128)(2,1)S(1)}, u32[]{:S(2)}, u32[]{:S(2)}) async-start(bf16[2,80,512]{2,1,0:T(8,128)(2,1)} %bitcast.10), calls=%async_computation | async-start | bytes 327680 | tf_op jit(solution)/shard_map/all_to_all | solution.py:126
  51.7 0.0 all-gather.6.cloned.1.call-start
  51.7 0.0 copy-done.4
  51.7 3.8 %all-to-all-done = bf16[2,80,512]{2,1,0:T(8,128)(2,1)S(1)} async-done(((bf16[2,80,512]{2,1,0:T(8,128)(2,1)}), bf16[2,80,512]{2,1,0:T(8,128)(2,1)S(1)}, u32[]{:S(2)}, u32[]{:S(2)}) %all-to-all-start) | async-done | bytes 163872 | tf_op jit(solution)/shard_map/all_to_all | solution.py:126
  55.6 0.0 copy-done.2
  55.6 0.0 copy-start.5
  55.6 0.0 copy-start.6
  55.6 3.2 %multiply_reduce_fusion = (f32[80]{0:T(128)S(1)}, f32[80,2048]{1,0:T(8,128)S(1)}) fusion(bf16[80,1024]{1,0:T(8,128)(2,1)S(1)} %bitcast.54, bf16[1024,2048]{1,0:T(8,128)(2,1)} %param.23, bf16[80,2048]{1,0:T(8,128)(2,1)S(1)} %copy-done.2), kind=kOutput, calls=%fused_computation.51 | convolution fusion | flops 336527296 | bytes 5341504 | tf_op jit(solution)/shard_map/dot_general | solution.py:134
  58.8 0.9 multiply_convert_fusion.1
  59.7 0.0 all-gather.6.cloned.1.call-update
  59.7 0.0 reduce-scatter.2.cloned.1.call-start
  59.7 0.0 copy-done.5
  59.8 23.9 %all-gather = f32[16,80,8]{1,2,0:T(8,128)S(1)} all-gather(f32[1,80,8]{1,2,0:T(8,128)S(1)} %bitcast.57), channel_id=1, replica_groups=mesh['grp'=2,'sp'=8,'tp'=2] {'sp','tp'}, dimensions={0}, use_global_device_ids=true | all-gather | bytes 43520 | tf_op jit(solution)/shard_map/all_gather | solution.py:90
  83.7 0.1 reshape.193
  83.8 0.1 select_reduce_fusion
  83.9 31.4 %all-gather.6.cloned.1.call-done = bf16[1280,2048]{1,0:T(8,128)(2,1)} async-done(((bf16[80,2048]{1,0:T(8,128)(2,1)}), bf16[1280,2048]{1,0:T(8,128)(2,1)}) %all-gather.6.cloned.1.call-update) | async-done | bytes 5242896 | tf_op jit(solution)/shard_map/all_gather | solution.py:137
  115.2 7.6 %convolution_minimum_fusion = f32[1280,512]{1,0:T(8,128)} fusion(bf16[1280,2048]{1,0:T(8,128)(2,1)} %all-gather.6.cloned.1.call-done, bf16[1,2048,512]{2,1,0:T(8,128)(2,1)} %param.25), kind=kOutput, calls=%fused_computation.2 | convolution fusion | flops 2685009920 | bytes 9961472 | tf_op jit(solution)/shard_map/dot_general | solution.py:53
  122.8 10.5 %multiply_convert_fusion = bf16[1280,2048]{1,0:T(8,128)(2,1)} fusion(f32[1280]{0:T(1024)S(1)} %select_reduce_fusion, bf16[1,512,2048]{2,1,0:T(8,128)(2,1)S(1)} %copy-done, f32[1280,512]{1,0:T(8,128)} %convolution_minimum_fusion, bf16[1280,2048]{1,0:T(8,128)(2,1)} %all-gather.6.cloned.1.call-done, bf16[1,2048,512]{2,1,0:T(8,128)(2,1)} %param.26), kind=kOutput, calls=%fused_computation | convolution fusion | flops 5379850240 | bytes 17306624 | tf_op jit(solution)/shard_map/dot_general | solution.py:139
  133.3 0.0 reduce-scatter.2.cloned.1.call-update
  133.3 74.7 %reduce-scatter.2.cloned.1.call-done = bf16[80,2048]{1,0:T(8,128)(2,1)} async-done(((bf16[1280,2048]{1,0:T(8,128)(2,1)}), bf16[80,2048]{1,0:T(8,128)(2,1)}) %reduce-scatter.2.cloned.1.call-update) | async-done | bytes 327696 | tf_op jit(solution)/shard_map/reduce_scatter | solution.py:143
  208.0 1.8 add_convert_fusion
  (15 shorter events, 0.2 us)
Async XLA Ops:
  6.5 116.3 %copy-start = (bf16[1,512,2048]{2,1,0:T(8,128)(2,1)S(1)}, bf16[1,512,2048]{2,1,0:T(8,128)(2,1)}, u32[]{:S(2)}) copy-start(bf16[1,512,2048]{2,1,0:T(8,128)(2,1)} %param.27) | copy-start | bytes 6291460
  6.5 32.4 %copy-start.7 = (bf16[512,512]{1,0:T(8,128)(2,1)S(1)}, bf16[512,512]{1,0:T(8,128)(2,1)}, u32[]{:S(2)}) copy-start(bf16[512,512]{1,0:T(8,128)(2,1)} %param.20) | copy-start | bytes 1572868
  6.5 32.4 %all-gather.4.cloned.1.call-start = ((), (), s32[]{:S(2)}) async-start(), calls=%async_computation.2 | async-start | bytes 1843200 | tf_op jit(solution)/shard_map/all_gather | solution.py:89
  12.9 28.3 %copy-start.3 = (bf16[160,512]{1,0:T(8,128)(2,1)S(1)}, bf16[160,512]{1,0:T(8,128)(2,1)}, u32[]{:S(2)}) copy-start(bf16[160,512]{1,0:T(8,128)(2,1)} %param.15) | copy-start | bytes 491524
  41.1 1.4 copy-start.1
  42.0 1.3 copy-start.8
  46.5 5.2 %copy-start.4 = (bf16[2048]{0:T(1024)(128)(2,1)S(1)}, bf16[2048]{0:T(1024)(128)(2,1)}, u32[]{:S(2)}) copy-start(bf16[2048]{0:T(1024)(128)(2,1)} %param.24) | copy-start | bytes 12292
  46.5 9.1 %copy-start.2 = (bf16[80,2048]{1,0:T(8,128)(2,1)S(1)}, bf16[80,2048]{1,0:T(8,128)(2,1)}, u32[]{:S(2)}) copy-start(bf16[80,2048]{1,0:T(8,128)(2,1)} %param.22) | copy-start | bytes 983044
  48.2 7.3 %all-to-all-start = ((bf16[2,80,512]{2,1,0:T(8,128)(2,1)}), bf16[2,80,512]{2,1,0:T(8,128)(2,1)S(1)}, u32[]{:S(2)}, u32[]{:S(2)}) async-start(bf16[2,80,512]{2,1,0:T(8,128)(2,1)} %bitcast.10), calls=%async_computation | async-start | bytes 327680 | tf_op jit(solution)/shard_map/all_to_all | solution.py:126
  51.7 63.6 %all-gather.6.cloned.1.call-start = ((), (), s32[]{:S(2)}) async-start(), calls=%async_computation.3 | async-start | bytes 5570560 | tf_op jit(solution)/shard_map/all_gather | solution.py:137
  55.6 4.2 %copy-start.5 = (f32[80,4]{0,1:T(4,128)S(1)}, f32[80,4]{0,1:T(4,128)}, u32[]{:S(2)}) copy-start(f32[80,4]{0,1:T(4,128)} %param.29) | copy-start | bytes 3844
  55.6 4.2 %copy-start.6 = (s32[80,4]{0,1:T(4,128)S(1)}, s32[80,4]{0,1:T(4,128)}, u32[]{:S(2)}) copy-start(s32[80,4]{0,1:T(4,128)} %param.28) | copy-start | bytes 3844
  59.7 148.3 %reduce-scatter.2.cloned.1.call-start = ((), (), s32[]{:S(2)}) async-start(), calls=%async_computation.4 | async-start | bytes 5570560 | tf_op jit(solution)/shard_map/reduce_scatter | solution.py:143
Sparse Core Ops, SparseCore 0:
  11.9 27.0 all-gather.3
  59.8 55.3 all-gather.5
  133.4 74.5 reduce-scatter.1

commit v2 on v1

--- a/solution.py
+++ b/solution.py
@@ -1,6 +1,10 @@
+import functools
+
 import jax
 import jax.numpy as jnp
 from jax import lax
+from jax.experimental import pallas as pl
+from jax.experimental.pallas import tpu as pltpu
 from jax.sharding import PartitionSpec as P
 
 PLAIN_HEAD_WIDTH = 128
@@ -13,6 +17,8 @@
 eps = 1e-06
 limit = 7.0
 slope = 1.702
+CORES = 2
+VMEM_BYTES = 60 * 2**20
 
 
 def turn(vector, row_shift, col_shift):
@@ -53,6 +59,280 @@
     gate_pre = jnp.minimum(jnp.dot(rows, gate_w, preferred_element_type=jnp.float32), limit)
     up_pre = jnp.clip(jnp.dot(rows, up_w, preferred_element_type=jnp.float32), -limit, limit)
     return ((up_pre + 1.0) * gate_pre * jax.nn.sigmoid(slope * gate_pre)).astype(jnp.bfloat16)
+
+
+def flipped(index, mask):
+    out = index
+    bit = 1
+    while bit <= mask:
+        if mask & bit:
+            out = out + bit - 2 * bit * ((index // bit) % 2)
+        bit *= 2
+    return out
+
+
+def experts_kernel(
+    chips,
+    group,
+    rows_ref,
+    hidden_ref,
+    share_ref,
+    gate_hbm,
+    up_hbm,
+    down_hbm,
+    out_ref,
+    gathered,
+    partial,
+    from_core,
+    from_tp,
+    from_chip,
+    gate_ref,
+    up_ref,
+    down_ref,
+    load_sem,
+    z_send,
+    z_recv,
+    x_send,
+    x_recv,
+    c_send,
+    c_recv,
+    rc_send,
+    rc_recv,
+    rx_send,
+    rx_recv,
+    rz_send,
+    rz_recv,
+):
+    place = lax.axis_index("sp")
+    column = lax.axis_index("tp")
+    chip, core = place // CORES, place % CORES
+    rows_dev, model_width = rows_ref.shape
+    per_chip = CORES * group
+
+    def other(index, shift):
+        return (index + shift) % group
+
+    def slot(k, core_at, column_at):
+        return flipped(chip, k) * per_chip + core_at * group + column_at
+
+    partner = {"sp": chip * CORES + 1 - core}
+
+    def chip_peer(k):
+        return {"sp": flipped(chip, k) * CORES + core}
+
+    barrier = pltpu.get_barrier_semaphore()
+    pl.semaphore_signal(barrier, inc=1, device_id=partner)
+    for k in range(1, chips):
+        pl.semaphore_signal(barrier, inc=1, device_id=chip_peer(k))
+    for shift in range(1, group):
+        pl.semaphore_signal(barrier, inc=1, device_id={"tp": other(column, shift)})
+    loads = [
+        pltpu.make_async_copy(src, dst, load_sem.at[i])
+        for i, (src, dst) in enumerate(
+            ((gate_hbm, gate_ref), (up_hbm, up_ref), (down_hbm, down_ref))
+        )
+    ]
+    for load in loads:
+        load.start()
+    pl.semaphore_wait(barrier, chips + group - 1)
+
+    sends = []
+
+    def remote(src, dst, send_sem, recv_sem, device):
+        return pltpu.make_async_remote_copy(
+            src_ref=src, dst_ref=dst, send_sem=send_sem, recv_sem=recv_sem, device_id=device
+        )
+
+    def launch(copy):
+        copy.start()
+        sends.append(copy)
+
+    def source(k, back):
+        if k == 0 and back == 0:
+            return rows_ref
+        return gathered.at[slot(k, core, other(column, group - back))]
+
+    def chip_copy(k):
+        return remote(
+            rows_ref, gathered.at[slot(0, core, column)], z_send.at[k], z_recv.at[k], chip_peer(k)
+        )
+
+    def chip_wait(k):
+        landed = gathered.at[slot(k, core, column)]
+        remote(landed, landed, z_send.at[k], z_recv.at[k], chip_peer(k)).wait_recv()
+
+    def tp_copy(k, shift):
+        return remote(
+            source(k, 0),
+            gathered.at[slot(k, core, column)],
+            x_send.at[k, shift],
+            x_recv.at[k, shift],
+            {"tp": other(column, shift)},
+        )
+
+    def tp_wait(k, shift):
+        landed = gathered.at[slot(k, core, other(column, group - shift))]
+        remote(
+            landed,
+            landed,
+            x_send.at[k, shift],
+            x_recv.at[k, shift],
+            {"tp": other(column, shift)},
+        ).wait_recv()
+
+    def core_copy(k, back):
+        return remote(
+            source(k, back),
+            gathered.at[slot(k, core, other(column, group - back))],
+            c_send.at[k, back],
+            c_recv.at[k, back],
+            partner,
+        )
+
+    def core_wait(k, back):
+        landed = gathered.at[slot(k, 1 - core, other(column, group - back))]
+        remote(landed, landed, c_send.at[k, back], c_recv.at[k, back], partner).wait_recv()
+
+    def spread(k):
+        for shift in range(1, group):
+            launch(tp_copy(k, shift))
+        launch(core_copy(k, 0))
+
+    def compute(k):
+        first = flipped(chip, k) * per_chip
+        rows = gathered[pl.ds(first, per_chip)].reshape(per_chip * rows_dev, model_width)
+        active = expert_active(rows, gate_ref[...], up_ref[...])
+        share = share_ref[pl.ds(first, per_chip)].reshape(per_chip * rows_dev, 1)
+        product = jnp.dot(active, down_ref[...], preferred_element_type=jnp.float32)
+        partial[pl.ds(first, per_chip)] = (
+            (product * share).astype(jnp.bfloat16).reshape(per_chip, rows_dev, model_width)
+        )
+
+    def partner_copy(k):
+        return remote(
+            partial.at[pl.ds(slot(k, 1 - core, 0), group)],
+            from_core.at[k],
+            rc_send.at[k],
+            rc_recv.at[k],
+            partner,
+        )
+
+    def sum_cores(k):
+        partner_copy(k).wait_recv()
+        first = slot(k, core, 0)
+        partial[pl.ds(first, group)] = (
+            partial[pl.ds(first, group)].astype(jnp.float32) + from_core[k].astype(jnp.float32)
+        ).astype(jnp.bfloat16)
+        for shift in range(1, group):
+            launch(tp_sum_copy(k, shift))
+
+    def tp_sum_copy(k, shift):
+        return remote(
+            partial.at[slot(k, core, other(column, shift))],
+            from_tp.at[k, shift - 1],
+            rx_send.at[k, shift],
+            rx_recv.at[k, shift],
+            {"tp": other(column, shift)},
+        )
+
+    def chip_sum_copy(k):
+        return remote(
+            partial.at[slot(k, core, column)],
+            from_chip.at[k],
+            rz_send.at[k],
+            rz_recv.at[k],
+            chip_peer(k),
+        )
+
+    def sum_tp(k):
+        total = partial[slot(k, core, column)].astype(jnp.float32)
+        for shift in range(1, group):
+            tp_sum_copy(k, shift).wait_recv()
+            total = total + from_tp[k, shift - 1].astype(jnp.float32)
+        if k == 0:
+            out_ref[...] = (hidden_ref[...].astype(jnp.float32) + total)
+            return
+        partial[slot(k, core, column)] = total.astype(jnp.bfloat16)
+        launch(chip_sum_copy(k))
+
+    spread(0)
+    for k in range(1, chips):
+        launch(chip_copy(k))
+    gathered[slot(0, core, column)] = rows_ref[...]
+    for k in range(chips + 2):
+        if k < chips:
+            for shift in range(1, group):
+                tp_wait(k, shift)
+                launch(core_copy(k, shift))
+            if k + 1 < chips:
+                chip_wait(k + 1)
+                spread(k + 1)
+            for back in range(group):
+                core_wait(k, back)
+            if k == 0:
+                for load in loads:
+                    load.wait()
+            compute(k)
+            launch(partner_copy(k))
+        if 0 <= k - 1 < chips:
+            sum_cores(k - 1)
+        if 0 <= k - 2 < chips:
+            sum_tp(k - 2)
+    for k in range(1, chips):
+        chip_sum_copy(k).wait_recv()
+        out_ref[...] += from_chip[k].astype(jnp.float32)
+    for copy in sends:
+        copy.wait_send()
+
+
+def run_experts(rows, hidden, shares, gate_w, up_w, down_w):
+    group = lax.axis_size("tp")
+    chips = lax.axis_size("sp") // CORES
+    rows_dev, model_width = rows.shape
+    blocks = chips * CORES * group
+    dma = pltpu.SemaphoreType.DMA
+    block = (rows_dev, model_width)
+    whole = pl.BlockSpec(memory_space=pltpu.VMEM)
+    return pl.pallas_call(
+        functools.partial(experts_kernel, chips, group),
+        out_shape=jax.ShapeDtypeStruct(block, jnp.float32),
+        in_specs=[whole] * 3 + [pl.BlockSpec(memory_space=pl.ANY)] * 3,
+        out_specs=whole,
+        scratch_shapes=[
+            pltpu.VMEM((blocks,) + block, jnp.bfloat16),
+            pltpu.VMEM((blocks,) + block, jnp.bfloat16),
+            pltpu.VMEM((chips, group) + block, jnp.bfloat16),
+            pltpu.VMEM((chips, group - 1) + block, jnp.bfloat16),
+            pltpu.VMEM((chips,) + block, jnp.bfloat16),
+            pltpu.VMEM(gate_w.shape, jnp.bfloat16),
+            pltpu.VMEM(up_w.shape, jnp.bfloat16),
+            pltpu.VMEM(down_w.shape, jnp.bfloat16),
+            dma((3,)),
+            dma((chips,)),
+            dma((chips,)),
+            dma((chips, group)),
+            dma((chips, group)),
+            dma((chips, group)),
+            dma((chips, group)),
+            dma((chips,)),
+            dma((chips,)),
+            dma((chips, group)),
+            dma((chips, group)),
+            dma((chips,)),
+            dma((chips,)),
+        ],
+        compiler_params=pltpu.CompilerParams(
+            collective_id=0, has_side_effects=True, vmem_limit_bytes=VMEM_BYTES
+        ),
+    )(rows, hidden, shares.reshape(blocks, rows_dev, 1), gate_w, up_w, down_w)
+
+
+def experts_fit(rows_dev, model_width):
+    group, places = lax.axis_size("tp"), lax.axis_size("sp")
+    chips = places // CORES
+    if group < 2 or places % CORES or chips & (chips - 1) or rows_dev % 16:
+        return False
+    return 3 * places * group * rows_dev * model_width * 2 < VMEM_BYTES // 2
 
 
 def on_device(
@@ -134,12 +414,16 @@
     projected = jnp.dot(own_rows, out_weight, preferred_element_type=jnp.float32)
     hidden = (residual.astype(jnp.float32) + projected).astype(jnp.bfloat16)
     normed = norm_scale(hidden, ffn_gain).astype(jnp.bfloat16)
+    own_share = jnp.sum(
+        jnp.where(expert_ids[None, :] == lax.axis_index("sp"), shares, 0.0), axis=1, keepdims=True
+    )
+    if experts_fit(rows_dev, residual.shape[1]):
+        return run_experts(
+            normed, hidden, own_share, gate_weight[0], up_weight[0], down_weight[0]
+        ).astype(jnp.bfloat16)
     rows = lax.all_gather(normed, ("sp", "tp"), axis=0, tiled=True)
     active = expert_active(rows, gate_weight[0], up_weight[0])
     product = jnp.dot(active, down_weight[0], preferred_element_type=jnp.float32)
-    own_share = jnp.sum(
-        jnp.where(expert_ids[None, :] == lax.axis_index("sp"), shares, 0.0), axis=1, keepdims=True
-    )
     mixture = lax.psum_scatter(
         (own_share * product).astype(jnp.bfloat16),
         ("sp", "tp"),

time: 220 us -> 163 us (0.74); the launches traced: 216 us -> 162 us
  waiting for transfers between devices: 136 us -> 2.53 us
  Pallas kernels: 0 us -> 93.2 us
  matrix products: 28.3 us -> 10.2 us
  blocking collectives: 23.9 us -> 26.3 us
    pallas_call x0 -> x1, Pallas kernels: none -> 93.2 us  [run_experts(): pl.pallas_call(functools.partial(experts_kernel, chips, group), out_shape...]
    reduce_scatter x1 -> x0, waiting for transfers between devices: 74.7 us -> none  [on_device(): lax.psum_scatter((own_share * product).astype(jnp.bfloat16), ('sp', 'tp')...]
    all_gather x1 -> x0, waiting for transfers between devices: 31.4 us -> none  [on_device(): rows = lax.all_gather(normed, ('sp', 'tp'), axis=0, tiled=True)]
    all_gather x1, waiting for transfers between devices: 26.1 us -> 0.61 us  [on_device(): everyone = lax.all_gather(sent, 'sp', axis=0, tiled=True)]
    dot_general x2 -> x0, matrix products: 18 us -> none  [the longest x1 10.5 us: on_device(): jnp.dot(active, down_weight[0], preferred_element_type=jnp.float32)]
    all_gather x1, blocking collectives: 23.9 us -> 26.3 us  [on_device(): shares = lax.all_gather(share, ('sp', 'tp'), axis=0, tiled=True)]
  transfers between devices with their start and end apart: 4 -> 2, of which waited for: 4 -> 2; matrix products, arithmetic and copies ran while one was open for 1% -> 1% of each run, Pallas kernels for 0% -> 0%
where the time goes in v2:
time: 163 us; the launch traced here: 162 us
  Pallas kernels  93.2 us (57%)
  blocking collectives  26.3 us (16%)
  between operations  13.7 us (8%)
  matrix products  10.2 us (6%)
  other arithmetic  8.49 us (5%)
  local copies, waits for them, and re-layouts  4.07 us (2%)
  starting transfers between devices  3.64 us (2%)
  waiting for transfers between devices  2.53 us (2%)
    pallas_call x1, Pallas kernels, run_experts(): pl.pallas_call(functools.partial(experts_kernel, chips, group), out_shape...  93.2 us
    all_gather x1, blocking collectives, on_device(): shares = lax.all_gather(share, ('sp', 'tp'), axis=0, tiled=True)  26.3 us
    all_to_all x1, starting transfers between devices, on_device(): lax.all_to_all(attended.reshape(group, rows_dev, heads_dev * VALUE_WIDTH)...  3.61 us
  transfers between devices with their start and end apart: 2, of which 2 were waited for; matrix products, arithmetic and copies ran while one was open for 1% of the time, Pallas kernels for 0%

profile of v2, /device:TPU:9, one launch (start us, length us, event | category | flops | bytes accessed | tf_op | source)
XLA Modules:
  0.0 162.2 jit_solution(16153976530136592754)
XLA Ops:
  6.5 0.0 copy-start
  6.5 0.0 copy-start.5
  6.5 0.0 copy-start.6
  6.5 0.0 copy-start.8
  6.5 0.0 copy-start.7
  6.5 0.0 all-gather.3.cloned.1.call-start
  6.6 0.8 convert_element_type.84
  7.5 0.2 multiply_cosine_fusion
  7.7 0.1 copy.54
  7.8 0.1 copy.55
  7.9 0.1 copy.56
  8.0 0.1 copy.57
  8.1 1.0 fusion.30
  9.2 0.7 convert_element_type.82
  9.9 1.0 fusion.32
  10.9 0.8 concatenate.13
  11.7 0.0 all-gather.3.cloned.1.call-update
  11.7 0.0 copy-done.5
  11.7 0.1 copy.58
  11.9 0.0 copy-done.6
  11.9 0.0 copy-done.8
  11.9 0.0 copy-done.7
  11.9 26.3 %all-gather = f32[16,80,8]{1,2,0:T(8,128)S(1)} all-gather(f32[1,80,8]{1,2,0:T(8,128)S(1)} %bitcast.50), channel_id=1, replica_groups=mesh['grp'=2,'sp'=8,'tp'=2] {'sp','tp'}, dimensions={0}, use_global_device_ids=true | all-gather | bytes 43520 | tf_op jit(solution)/shard_map/all_gather | solution.py:370
  38.3 0.1 reshape.192
  38.5 0.0 copy-start.4
  38.5 0.6 all-gather.3.cloned.1.call-done
  39.1 0.0 copy-done
  39.1 2.1 %convolution_convert_fusion.1 = bf16[1280,512]{1,0:T(8,128)(2,1)S(1)} fusion(bf16[512,512]{1,0:T(8,128)(2,1)S(1)} %copy-done, bf16[1280,576]{1,0:T(8,128)(2,1)} %all-gather.3.cloned.1.call-done), kind=kOutput, calls=%fused_computation.1 | convolution fusion | flops 671744000 | bytes 3145728 | tf_op jit(solution)/shard_map/dot_general | solution.py:373
  41.3 0.0 copy-done.4
  41.3 0.3 convolution_bitcast_fusion.3
  41.5 0.3 convolution_bitcast_fusion.2
  41.8 0.0 copy-start.2
  41.8 0.3 convolution_bitcast_fusion.1
  42.1 0.3 convolution_bitcast_fusion
  42.4 0.9 copy-done.2
  43.2 0.0 copy-start.9
  43.2 0.4 fusion.55
  43.6 0.3 fusion.11
  43.9 0.4 copy-done.9
  44.3 0.8 convolution_convert_fusion
  45.1 0.3 fusion.7
  45.5 0.4 fusion.54
  45.9 0.3 fusion.13
  46.1 0.3 fusion.8
  46.5 0.4 fusion.53
  46.9 0.3 fusion.15
  47.2 0.3 fusion.9
  47.5 0.4 fusion.52
  47.9 0.3 fusion.17
  48.2 0.0 copy-start.3
  48.2 0.3 fusion.10
  48.5 0.7 pad_maximum_fusion
  49.2 3.6 %all-to-all-start = ((bf16[2,80,512]{2,1,0:T(8,128)(2,1)}), bf16[2,80,512]{2,1,0:T(8,128)(2,1)S(1)}, u32[]{:S(2)}, u32[]{:S(2)}) async-start(bf16[2,80,512]{2,1,0:T(8,128)(2,1)} %bitcast.10), calls=%async_computation | async-start | bytes 327680 | tf_op jit(solution)/shard_map/all_to_all | solution.py:406
  52.8 0.1 select_reduce_fusion
  52.9 1.3 reshape_broadcast_in_dim.4.share_ref
  54.2 1.9 %all-to-all-done = bf16[2,80,512]{2,1,0:T(8,128)(2,1)S(1)} async-done(((bf16[2,80,512]{2,1,0:T(8,128)(2,1)}), bf16[2,80,512]{2,1,0:T(8,128)(2,1)S(1)}, u32[]{:S(2)}, u32[]{:S(2)}) %all-to-all-start) | async-done | bytes 163872 | tf_op jit(solution)/shard_map/all_to_all | solution.py:406
  56.2 0.0 copy-done.3
  56.2 3.2 %fusion.19 = (f32[80]{0:T(128)S(1)}, bf16[80,2048]{1,0:T(8,128)(2,1)S(1)}) fusion(bf16[80,1024]{1,0:T(8,128)(2,1)S(1)} %bitcast.48, bf16[1024,2048]{1,0:T(8,128)(2,1)} %param.23, bf16[80,2048]{1,0:T(8,128)(2,1)S(1)} %copy-done.3), kind=kOutput, calls=%fused_computation.40 | convolution fusion | flops 336527296 | bytes 5013824 | tf_op jit(solution)/shard_map/dot_general | solution.py:414
  59.3 0.0 copy-start.1
  59.4 0.9 fusion.21.rows_ref
  60.2 0.0 copy-done.1
  60.2 93.2 %shard_map.145 = f32[80,2048]{1,0:T(8,128)} custom-call(bf16[80,2048]{1,0:T(8,128)(2,1)} %fusion.21.rows_ref, bf16[80,2048]{1,0:T(8,128)(2,1)} %copy-done.1, f32[16,80,1]{2,1,0:T(8,128)} %reshape_broadcast_in_dim.4.share_ref, bf16[2048,512]{1,0:T(8,128)(2,1)} %bitcast.44, bf16[2048,512]{1,0:T(8,128)(2,1)} %bitcast.45, bf16[512,2048]{1,0:T(8,128)(2,1)} %bitcast.46), custom_call_target="tpu_custom_call" | custom-call | tf_op jit(solution)/shard_map/pallas_call | solution.py:296
  153.5 1.8 %convert_element_type.101 = bf16[80,2048]{1,0:T(8,128)(2,1)} convert(f32[80,2048]{1,0:T(8,128)} %shard_map.145) | non-fusion elementwise | flops 163840 | bytes 983040 | tf_op jit(solution)/shard_map/convert_element_type | solution.py:423
  (12 shorter events, 0.2 us)
Async XLA Ops:
  6.5 32.6 %copy-start = (bf16[512,512]{1,0:T(8,128)(2,1)S(1)}, bf16[512,512]{1,0:T(8,128)(2,1)}, u32[]{:S(2)}) copy-start(bf16[512,512]{1,0:T(8,128)(2,1)} %param.20) | copy-start | bytes 1572868
  6.5 5.2 %copy-start.5 = (bf16[160,256]{1,0:T(8,128)(2,1)S(1)}, bf16[160,256]{1,0:T(8,128)(2,1)}, u32[]{:S(2)}) copy-start(bf16[160,256]{1,0:T(8,128)(2,1)} %param.16) | copy-start | bytes 245764
  6.5 5.3 %copy-start.6 = (bf16[2048]{0:T(1024)(128)(2,1)S(1)}, bf16[2048]{0:T(1024)(128)(2,1)}, u32[]{:S(2)}) copy-start(bf16[2048]{0:T(1024)(128)(2,1)} %param.24) | copy-start | bytes 12292
  6.5 5.4 %copy-start.8 = (s32[80,4]{0,1:T(4,128)S(1)}, s32[80,4]{0,1:T(4,128)}, u32[]{:S(2)}) copy-start(s32[80,4]{0,1:T(4,128)} %param.28) | copy-start | bytes 3844
  6.5 5.4 %copy-start.7 = (f32[80,4]{0,1:T(4,128)S(1)}, f32[80,4]{0,1:T(4,128)}, u32[]{:S(2)}) copy-start(f32[80,4]{0,1:T(4,128)} %param.29) | copy-start | bytes 3844
  6.5 32.5 %all-gather.3.cloned.1.call-start = ((), (), s32[]{:S(2)}) async-start(), calls=%async_computation.1 | async-start | bytes 1843200 | tf_op jit(solution)/shard_map/all_gather | solution.py:369
  38.5 2.8 %copy-start.4 = (bf16[160,512]{1,0:T(8,128)(2,1)S(1)}, bf16[160,512]{1,0:T(8,128)(2,1)}, u32[]{:S(2)}) copy-start(bf16[160,512]{1,0:T(8,128)(2,1)} %param.15) | copy-start | bytes 491524
  41.8 1.4 copy-start.2
  43.2 1.0 copy-start.9
  48.2 8.0 %copy-start.3 = (bf16[80,2048]{1,0:T(8,128)(2,1)S(1)}, bf16[80,2048]{1,0:T(8,128)(2,1)}, u32[]{:S(2)}) copy-start(bf16[80,2048]{1,0:T(8,128)(2,1)} %param.22) | copy-start | bytes 983044
  49.2 6.9 %all-to-all-start = ((bf16[2,80,512]{2,1,0:T(8,128)(2,1)}), bf16[2,80,512]{2,1,0:T(8,128)(2,1)S(1)}, u32[]{:S(2)}, u32[]{:S(2)}) async-start(bf16[2,80,512]{2,1,0:T(8,128)(2,1)} %bitcast.10), calls=%async_computation | async-start | bytes 327680 | tf_op jit(solution)/shard_map/all_to_all | solution.py:406
  59.3 0.9 copy-start.1
Sparse Core Ops, SparseCore 0:
  11.9 27.1 all-gather.2

commit v3 on v2

v3 whole, which is shorter than its diff:
```python
import functools

import jax
import jax.numpy as jnp
from jax import lax
from jax.experimental import pallas as pl
from jax.experimental.pallas import tpu as pltpu
from jax.sharding import PartitionSpec as P

PLAIN_HEAD_WIDTH = 128
QK_ROPE = 64
VALUE_WIDTH = 128
GRID_W = 64


theta = 10000.0
eps = 1e-06
limit = 7.0
slope = 1.702
CORES = 2
VMEM_BYTES = 60 * 2**20


def turn(vector, row_shift, col_shift):
    width = vector.shape[-1]
    count = width // 4
    half = width // 2
    freqs = theta ** (-jnp.arange(count, dtype=jnp.float32) / count)
    extra = (1,) * (vector.ndim - 2)
    pieces = []
    for portion, shift in ((vector[..., :half], row_shift), (vector[..., half:], col_shift)):
        angle = (shift.astype(jnp.float32)[:, None] * freqs[None, :]).reshape(
            (shift.shape[0],) + extra + (count,)
        )
        lower = portion[..., :count]
        upper = portion[..., count:]
        pieces.append(
            jnp.concatenate(
                [
                    lower * jnp.cos(angle) - upper * jnp.sin(angle),
                    lower * jnp.sin(angle) + upper * jnp.cos(angle),
                ],
                axis=-1,
            )
        )
    return jnp.concatenate(pieces, axis=-1)


def norm_scale(values, gain):
    wide = values.astype(jnp.float32)
    return (
        wide
        * lax.rsqrt(jnp.mean(wide * wide, axis=-1, keepdims=True) + eps)
        * gain.astype(jnp.float32)
    )


def expert_active(rows, gate_w, up_w):
    gate_pre = jnp.minimum(jnp.dot(rows, gate_w, preferred_element_type=jnp.float32), limit)
    up_pre = jnp.clip(jnp.dot(rows, up_w, preferred_element_type=jnp.float32), -limit, limit)
    return ((up_pre + 1.0) * gate_pre * jax.nn.sigmoid(slope * gate_pre)).astype(jnp.bfloat16)


def flipped(index, mask):
    out = index
    bit = 1
    while bit <= mask:
        if mask & bit:
            out = out + bit - 2 * bit * ((index // bit) % 2)
        bit *= 2
    return out


def gatherer(chips, group, own, gathered, sems, launch):
    z_send, z_recv, x_send, x_recv, c_send, c_recv = sems
    place = lax.axis_index("sp")
    column = lax.axis_index("tp")
    chip, core = place // CORES, place % CORES
    per_chip = CORES * group
    partner = {"sp": chip * CORES + 1 - core}

    def other(shift):
        return (column + shift) % group

    def slot(k, core_at, column_at):
        return flipped(chip, k) * per_chip + core_at * group + column_at

    def chip_peer(k):
        return {"sp": flipped(chip, k) * CORES + core}

    def remote(src, dst, send_sem, recv_sem, device):
        return pltpu.make_async_remote_copy(
            src_ref=src, dst_ref=dst, send_sem=send_sem, recv_sem=recv_sem, device_id=device
        )

    def greet():
        barrier = pltpu.get_barrier_semaphore()
        pl.semaphore_signal(barrier, inc=1, device_id=partner)
        for k in range(1, chips):
            pl.semaphore_signal(barrier, inc=1, device_id=chip_peer(k))
        for shift in range(1, group):
            pl.semaphore_signal(barrier, inc=1, device_id={"tp": other(shift)})

    def met():
        pl.semaphore_wait(pltpu.get_barrier_semaphore(), chips + group - 1)

    def source(k, back):
        if k == 0 and back == 0:
            return own
        return gathered.at[slot(k, core, other(group - back))]

    def chip_wait(k):
        landed = gathered.at[slot(k, core, column)]
        remote(landed, landed, z_send.at[k], z_recv.at[k], chip_peer(k)).wait_recv()

    def core_copy(k, back):
        return remote(
            source(k, back),
            gathered.at[slot(k, core, other(group - back))],
            c_send.at[k, back],
            c_recv.at[k, back],
            partner,
        )

    def core_wait(k, back):
        landed = gathered.at[slot(k, 1 - core, other(group - back))]
        remote(landed, landed, c_send.at[k, back], c_recv.at[k, back], partner).wait_recv()

    def tp_copy(k, shift):
        return remote(
            source(k, 0),
            gathered.at[slot(k, core, column)],
            x_send.at[k, shift],
            x_recv.at[k, shift],
            {"tp": other(shift)},
        )

    def tp_wait(k, shift):
        landed = gathered.at[slot(k, core, other(group - shift))]
        remote(
            landed, landed, x_send.at[k, shift], x_recv.at[k, shift], {"tp": other(shift)}
        ).wait_recv()

    def spread(k):
        for shift in range(1, group):
            launch(tp_copy(k, shift))
        launch(core_copy(k, 0))

    def begin():
        for k in range(1, chips):
            launch(
                remote(
                    own,
                    gathered.at[slot(0, core, column)],
                    z_send.at[k],
                    z_recv.at[k],
                    chip_peer(k),
                )
            )
        spread(0)

    def step(k):
        for shift in range(1, group):
            tp_wait(k, shift)
            launch(core_copy(k, shift))
        if k + 1 < chips:
            chip_wait(k + 1)
            spread(k + 1)
        for back in range(group):
            core_wait(k, back)

    return greet, met, begin, step, slot, chip_peer, partner, other, remote


def gather_kernel(chips, group, own, gathered, *sems):
    sends = []

    def launch(copy):
        copy.start()
        sends.append(copy)

    greet, met, begin, step, slot = gatherer(chips, group, own, gathered, sems, launch)[:5]
    greet()
    met()
    begin()
    gathered[slot(0, lax.axis_index("sp") % CORES, lax.axis_index("tp"))] = own[...]
    for k in range(chips):
        step(k)
    for copy in sends:
        copy.wait_send()


def gather_sems(chips, group):
    dma = pltpu.SemaphoreType.DMA
    return [dma((chips,))] * 2 + [dma((chips, group))] * 4


def run_gather(rows):
    group = lax.axis_size("tp")
    chips = lax.axis_size("sp") // CORES
    whole = pl.BlockSpec(memory_space=pltpu.VMEM)
    return pl.pallas_call(
        functools.partial(gather_kernel, chips, group),
        out_shape=jax.ShapeDtypeStruct((chips * CORES * group,) + rows.shape, rows.dtype),
        in_specs=[whole],
        out_specs=whole,
        scratch_shapes=gather_sems(chips, group),
        compiler_params=pltpu.CompilerParams(
            collective_id=1, has_side_effects=True, vmem_limit_bytes=VMEM_BYTES // 2
        ),
    )(rows)


def experts_kernel(
    chips,
    group,
    attended_ref,
    residual_ref,
    gain_ref,
    share_ref,
    out_hbm,
    gate_hbm,
    up_hbm,
    down_hbm,
    out_ref,
    heads,
    hidden,
    rows_ref,
    total_ref,
    gathered,
    partial,
    from_core,
    from_tp,
    from_chip,
    outw_ref,
    gate_ref,
    up_ref,
    down_ref,
    load_sem,
    h_send,
    h_recv,
    rc_send,
    rc_recv,
    rx_send,
    rx_recv,
    rz_send,
    rz_recv,
    *sems,
):
    column = lax.axis_index("tp")
    core = lax.axis_index("sp") % CORES
    rows_dev, model_width = rows_ref.shape
    per_chip = CORES * group
    sends = []

    def launch(copy):
        copy.start()
        sends.append(copy)

    greet, met, begin, step, slot, chip_peer, partner, other, remote = gatherer(
        chips, group, rows_ref, gathered, sems, launch
    )
    greet()
    loads = [
        pltpu.make_async_copy(src, dst, load_sem.at[i])
        for i, (src, dst) in enumerate(
            (
                (out_hbm, outw_ref),
                (gate_hbm, gate_ref),
                (up_hbm, up_ref),
                (down_hbm, down_ref),
            )
        )
    ]
    for load in loads:
        load.start()
    met()

    def heads_copy(shift):
        return remote(
            attended_ref.at[other(shift)],
            heads.at[column],
            h_send.at[shift],
            h_recv.at[shift],
            {"tp": other(shift)},
        )

    def heads_wait(shift):
        landed = heads.at[other(group - shift)]
        remote(
            landed, landed, h_send.at[shift], h_recv.at[shift], {"tp": other(shift)}
        ).wait_recv()

    for shift in range(1, group):
        launch(heads_copy(shift))
    heads[column] = attended_ref[column]
    loads[0].wait()
    for shift in range(1, group):
        heads_wait(shift)
    joined = jnp.concatenate([heads[at] for at in range(group)], axis=1)
    projected = jnp.dot(joined, outw_ref[...], preferred_element_type=jnp.float32)
    mixed = (residual_ref[...].astype(jnp.float32) + projected).astype(jnp.bfloat16)
    normed = norm_scale(mixed, gain_ref[...]).astype(jnp.bfloat16)
    rows_ref[...] = normed
    gathered[slot(0, core, column)] = normed
    hidden[...] = mixed
    begin()

    def compute(k):
        first = slot(k, 0, 0)
        rows = gathered[pl.ds(first, per_chip)].reshape(per_chip * rows_dev, model_width)
        active = expert_active(rows, gate_ref[...], up_ref[...])
        share = share_ref[pl.ds(first, per_chip)].reshape(per_chip * rows_dev, 1)
        product = jnp.dot(active, down_ref[...], preferred_element_type=jnp.float32)
        partial[pl.ds(first, per_chip)] = (
            (product * share).astype(jnp.bfloat16).reshape(per_chip, rows_dev, model_width)
        )

    def partner_copy(k):
        return remote(
            partial.at[pl.ds(slot(k, 1 - core, 0), group)],
            from_core.at[k],
            rc_send.at[k],
            rc_recv.at[k],
            partner,
        )

    def tp_sum_copy(k, shift):
        return remote(
            partial.at[slot(k, core, other(shift))],
            from_tp.at[k, shift - 1],
            rx_send.at[k, shift],
            rx_recv.at[k, shift],
            {"tp": other(shift)},
        )

    def chip_sum_copy(k):
        return remote(
            partial.at[slot(k, core, column)],
            from_chip.at[k],
            rz_send.at[k],
            rz_recv.at[k],
            chip_peer(k),
        )

    def sum_cores(k):
        partner_copy(k).wait_recv()
        first = slot(k, core, 0)
        partial[pl.ds(first, group)] = (
            partial[pl.ds(first, group)].astype(jnp.float32) + from_core[k].astype(jnp.float32)
        ).astype(jnp.bfloat16)
        for shift in range(1, group):
            launch(tp_sum_copy(k, shift))

    def sum_tp(k):
        total = partial[slot(k, core, column)].astype(jnp.float32)
        for shift in range(1, group):
            tp_sum_copy(k, shift).wait_recv()
            total = total + from_tp[k, shift - 1].astype(jnp.float32)
        if k == 0:
            total_ref[...] = hidden[...].astype(jnp.float32) + total
            return
        partial[slot(k, core, column)] = total.astype(jnp.bfloat16)
        launch(chip_sum_copy(k))

    for k in range(chips + 2):
        if k < chips:
            step(k)
            if k == 0:
                for load in loads[1:]:
                    load.wait()
            compute(k)
            launch(partner_copy(k))
        if 0 <= k - 1 < chips:
            sum_cores(k - 1)
        if 0 <= k - 2 < chips:
            sum_tp(k - 2)
    total = total_ref[...]
    for k in range(1, chips):
        chip_sum_copy(k).wait_recv()
        total = total + from_chip[k].astype(jnp.float32)
    out_ref[...] = total.astype(jnp.bfloat16)
    for copy in sends:
        copy.wait_send()


def run_experts(attended, residual, gain, shares, out_w, gate_w, up_w, down_w):
    group = lax.axis_size("tp")
    chips = lax.axis_size("sp") // CORES
    rows_dev, model_width = residual.shape
    blocks = chips * CORES * group
    dma = pltpu.SemaphoreType.DMA
    block = (rows_dev, model_width)
    heads = (group, rows_dev, attended.shape[1])
    whole = pl.BlockSpec(memory_space=pltpu.VMEM)
    return pl.pallas_call(
        functools.partial(experts_kernel, chips, group),
        out_shape=jax.ShapeDtypeStruct(block, jnp.bfloat16),
        in_specs=[whole] * 4 + [pl.BlockSpec(memory_space=pl.ANY)] * 4,
        out_specs=whole,
        scratch_shapes=[
            pltpu.VMEM(heads, jnp.bfloat16),
            pltpu.VMEM(block, jnp.bfloat16),
            pltpu.VMEM(block, jnp.bfloat16),
            pltpu.VMEM(block, jnp.float32),
            pltpu.VMEM((blocks,) + block, jnp.bfloat16),
            pltpu.VMEM((blocks,) + block, jnp.bfloat16),
            pltpu.VMEM((chips, group) + block, jnp.bfloat16),
            pltpu.VMEM((chips, group - 1) + block, jnp.bfloat16),
            pltpu.VMEM((chips,) + block, jnp.bfloat16),
            pltpu.VMEM(out_w.shape, jnp.bfloat16),
            pltpu.VMEM(gate_w.shape, jnp.bfloat16),
            pltpu.VMEM(up_w.shape, jnp.bfloat16),
            pltpu.VMEM(down_w.shape, jnp.bfloat16),
            dma((4,)),
            dma((group,)),
            dma((group,)),
            dma((chips,)),
            dma((chips,)),
            dma((chips, group)),
            dma((chips, group)),
            dma((chips,)),
            dma((chips,)),
        ]
        + gather_sems(chips, group),
        compiler_params=pltpu.CompilerParams(
            collective_id=0, has_side_effects=True, vmem_limit_bytes=VMEM_BYTES
        ),
    )(
        attended.reshape(heads),
        residual,
        gain.reshape(1, model_width),
        shares.reshape(blocks, rows_dev, 1),
        out_w,
        gate_w,
        up_w,
        down_w,
    )


def experts_fit(rows_dev, model_width):
    group, places = lax.axis_size("tp"), lax.axis_size("sp")
    chips = places // CORES
    if group < 2 or places % CORES or chips & (chips - 1) or rows_dev % 16:
        return False
    return 3 * places * group * rows_dev * model_width * 2 < VMEM_BYTES // 2


def on_device(
    query_plain,
    query_turn,
    latent,
    key_turn,
    latent_norm_scale,
    plain_key_matrix,
    value_matrix,
    residual,
    out_weight,
    ffn_gain,
    gate_weight,
    up_weight,
    down_weight,
    routes,
    route_weights,
):
    tok_dev = latent.shape[0]
    heads_dev = query_plain.shape[1] // PLAIN_HEAD_WIDTH
    model_width = residual.shape[1]
    place = lax.axis_index("sp") * tok_dev + jnp.arange(tok_dev, dtype=jnp.int32)
    grid_row = place // GRID_W
    grid_col = place % GRID_W
    rows_dev, model_width = residual.shape
    group = lax.axis_size("tp")
    count = lax.axis_size("sp")
    fits = experts_fit(rows_dev, model_width)
    expert_ids = jnp.arange(count, dtype=jnp.int32)
    share = jnp.sum(
        route_weights[..., None] * (routes[..., None] == expert_ids).astype(jnp.float32), axis=1
    )
    latent_width = latent.shape[1]
    wide = latent_width + QK_ROPE

    def key_side(latents, turns, at_row, at_col):
        normed_latent = norm_scale(latents, latent_norm_scale).astype(jnp.bfloat16)
        key_rot = turn(turns.astype(jnp.float32), at_row, at_col).astype(jnp.bfloat16)
        return [normed_latent, key_rot]

    if fits:
        first = lax.axis_index("tp") * rows_dev
        high = lax.reduce_precision(share, 8, 7)
        filled = wide + 2 * count
        sent = jnp.concatenate(
            key_side(
                lax.dynamic_slice_in_dim(latent, first, rows_dev, 0),
                lax.dynamic_slice_in_dim(key_turn, first, rows_dev, 0),
                lax.dynamic_slice_in_dim(grid_row, first, rows_dev, 0),
                lax.dynamic_slice_in_dim(grid_col, first, rows_dev, 0),
            )
            + [high.astype(jnp.bfloat16), (share - high).astype(jnp.bfloat16)]
            + [jnp.zeros((rows_dev, -filled % 128), jnp.bfloat16)],
            axis=1,
        )
        everyone = run_gather(sent)
        everyone = everyone.reshape(everyone.shape[0] * rows_dev, everyone.shape[2])
        shares = everyone[:, wide : wide + count].astype(jnp.float32) + everyone[
            :, wide + count : filled
        ].astype(jnp.float32)
    else:
        sent = jnp.concatenate(key_side(latent, key_turn, grid_row, grid_col), axis=1)
        everyone = lax.all_gather(sent, "sp", axis=0, tiled=True)
        shares = lax.all_gather(share, ("sp", "tp"), axis=0, tiled=True)
    own_share = jnp.sum(
        jnp.where(expert_ids[None, :] == lax.axis_index("sp"), shares, 0.0), axis=1, keepdims=True
    )
    all_latent = everyone[:, :latent_width]
    all_rot = everyone[:, latent_width:wide]
    keys = jnp.dot(all_latent, plain_key_matrix, preferred_element_type=jnp.float32).astype(
        jnp.bfloat16
    )
    values = jnp.dot(all_latent, value_matrix, preferred_element_type=jnp.float32).astype(
        jnp.bfloat16
    )
    query_rot = turn(
        query_turn.astype(jnp.float32).reshape(tok_dev, heads_dev, QK_ROPE), grid_row, grid_col
    ).astype(jnp.bfloat16)
    scale = (PLAIN_HEAD_WIDTH + QK_ROPE) ** (-0.5)
    attended = []
    for head in range(heads_dev):
        span = slice(head * PLAIN_HEAD_WIDTH, (head + 1) * PLAIN_HEAD_WIDTH)
        scores = (
            jnp.einsum(
                "qd,kd->qk", query_plain[:, span], keys[:, span], preferred_element_type=jnp.float32
            )
            + jnp.einsum(
                "qd,kd->qk", query_rot[:, head], all_rot, preferred_element_type=jnp.float32
            )
        ) * scale
        weights = jnp.exp(scores - jnp.max(scores, axis=1, keepdims=True))
        summed = jnp.dot(
            weights.astype(jnp.bfloat16),
            values[:, head * VALUE_WIDTH : (head + 1) * VALUE_WIDTH],
            preferred_element_type=jnp.float32,
        )
        attended.append(
            (summed / jnp.sum(weights, axis=1, keepdims=True)).astype(jnp.bfloat16)
        )
    attended = jnp.concatenate(attended, axis=1)
    if fits:
        return run_experts(
            attended,
            residual,
            ffn_gain,
            own_share,
            out_weight,
            gate_weight[0],
            up_weight[0],
            down_weight[0],
        )
    swapped = lax.all_to_all(
        attended.reshape(group, rows_dev, heads_dev * VALUE_WIDTH),
        "tp",
        split_axis=0,
        concat_axis=0,
        tiled=True,
    )
    own_rows = jnp.transpose(swapped, (1, 0, 2)).reshape(rows_dev, group * heads_dev * VALUE_WIDTH)
    projected = jnp.dot(own_rows, out_weight, preferred_element_type=jnp.float32)
    hidden = (residual.astype(jnp.float32) + projected).astype(jnp.bfloat16)
    normed = norm_scale(hidden, ffn_gain).astype(jnp.bfloat16)
    rows = lax.all_gather(normed, ("sp", "tp"), axis=0, tiled=True)
    active = expert_active(rows, gate_weight[0], up_weight[0])
    product = jnp.dot(active, down_weight[0], preferred_element_type=jnp.float32)
    mixture = lax.psum_scatter(
        (own_share * product).astype(jnp.bfloat16),
        ("sp", "tp"),
        scatter_dimension=0,
        tiled=True,
    )
    return (hidden.astype(jnp.float32) + mixture.astype(jnp.float32)).astype(jnp.bfloat16)


def solution(mesh):
    placed = (
        P(("grp", "sp"), "tp"),
        P(("grp", "sp"), "tp"),
        P(("grp", "sp"), None),
        P(("grp", "sp"), None),
        P(),
        P(None, "tp"),
        P(None, "tp"),
        P(("grp", "sp", "tp"), None),
        P(),
        P(),
        P("sp", None, "tp"),
        P("sp", None, "tp"),
        P("sp", "tp", None),
        P(("grp", "sp", "tp"), None),
        P(("grp", "sp", "tp"), None),
    )
    return jax.shard_map(
        on_device,
        mesh=mesh,
        in_specs=placed,
        out_specs=P(("grp", "sp", "tp"), None),
        check_vma=False,
    )
```

time: 163 us -> 133 us (0.82)
  blocking collectives: 26.3 us -> 0 us
  Pallas kernels: 93.2 us -> 113 us
  between operations: 13.7 us -> 0.21 us
  matrix products: 10.2 us -> 5.71 us
  starting transfers between devices: 3.64 us -> 0 us
  local copies, waits for them, and re-layouts: 4.07 us -> 7.08 us
  waiting for transfers between devices: 2.53 us -> 0 us
  other arithmetic: 8.49 us -> 6.42 us
    all_gather x1 -> x0, blocking collectives: 26.3 us -> none  [on_device(): shares = lax.all_gather(share, ('sp', 'tp'), axis=0, tiled=True)]
    pallas_call x0 -> x1, Pallas kernels: none -> 22.2 us  [run_gather(): pl.pallas_call(functools.partial(gather_kernel, chips, group), out_shape=...]
    all_to_all x1 -> x0, starting transfers between devices: 3.61 us -> none  [on_device(): lax.all_to_all(attended.reshape(group, rows_dev, heads_dev * VALUE_WIDTH)...]
    convert_element_type x4 -> x3, other arithmetic: 4.55 us -> 0.98 us  [the longest x1 0.97 us: key_side(): normed_latent = norm_scale(latents, latent_norm_scale).astype(jnp.bfloat16)]
    dot_general x1 -> x0, matrix products: 3.17 us -> none  [on_device(): jnp.dot(own_rows, out_weight, preferred_element_type=jnp.float32)]
    unnamed x22 -> x17, local copies, waits for them, and re-layouts: 1.46 us -> 3.87 us
    pallas_call x1, Pallas kernels: 93.2 us -> 91.1 us  [run_experts(): pl.pallas_call(functools.partial(experts_kernel, chips, group), out_shape...]
    all_to_all x1 -> x0, waiting for transfers between devices: 1.91 us -> none  [on_device(): lax.all_to_all(attended.reshape(group, rows_dev, heads_dev * VALUE_WIDTH)...]
  transfers between devices with their start and end apart: 2 -> 0, of which waited for: 2 -> 0; matrix products, arithmetic and copies ran while one was open for 1% -> 0% of each run, Pallas kernels for 0% -> 0%
where the time goes in v3:
time: 133 us
  Pallas kernels  113 us (85%)
  local copies, waits for them, and re-layouts  7.08 us (5%)
  other arithmetic  6.42 us (5%)
  matrix products  5.71 us (4%)
    pallas_call x1, Pallas kernels, run_experts(): pl.pallas_call(functools.partial(experts_kernel, chips, group), out_shape...  91.1 us
    pallas_call x1, Pallas kernels, run_gather(): pl.pallas_call(functools.partial(gather_kernel, chips, group), out_shape=...  22.2 us
    unnamed x17, local copies, waits for them, and re-layouts  3.87 us

profile of v3, /device:TPU:9, one launch (start us, length us, event | category | flops | bytes accessed | tf_op | source)
XLA Modules:
  0.0 132.7 jit_solution(17022851400084489113)
XLA Ops:
  0.0 0.0 copy-start
  0.0 0.1 dynamic-slice_convert_fusion
  0.1 0.9 constant_dynamic-slice_fusion
  1.0 0.1 copy.37
  1.1 0.4 fusion.52
  1.5 1.0 fusion.38
  2.5 0.7 convert_element_type.79
  3.2 1.0 fusion.40
  4.2 0.7 select_reduce_fusion.1
  4.9 0.1 copy.33
  5.0 0.1 copy.32
  5.1 0.1 copy.34
  5.2 0.1 concatenate.13.own
  5.4 22.2 %shard_map.145 = bf16[16,80,640]{2,1,0:T(8,128)(2,1)S(1)} custom-call(bf16[80,640]{1,0:T(8,128)(2,1)S(1)} %concatenate.13.own), custom_call_target="tpu_custom_call" | custom-call | tf_op jit(solution)/shard_map/pallas_call | solution.py:202
  27.6 0.0 copy-done
  27.6 0.0 copy-start.3
  27.6 0.8 convolution_convert_fusion.1
  28.5 0.0 copy-start.1
  28.5 1.1 copy-done.1
  29.5 0.0 copy-done.3
  29.5 0.0 copy-start.4
  29.5 0.3 convolution_bitcast_fusion.3
  29.8 0.2 multiply_cosine_fusion.3
  30.0 0.4 copy-done.4
  30.4 0.1 copy.35
  30.6 0.0 copy-start.6
  30.6 0.4 fusion.68
  31.0 0.3 fusion.10
  31.3 0.4 copy-done.6
  31.7 0.0 copy-start.2
  31.7 0.8 convolution_convert_fusion
  32.5 0.3 fusion.6
  32.9 0.1 copy-done.2
  33.0 0.3 convolution_bitcast_fusion.2
  33.3 0.4 fusion.67
  33.7 0.3 fusion.12
  33.9 0.3 fusion.7
  34.3 0.3 convolution_bitcast_fusion.1
  34.6 0.4 fusion.66
  35.0 0.3 fusion.14
  35.2 0.3 fusion.8
  35.6 0.3 convolution_bitcast_fusion
  35.9 0.4 fusion.65
  36.3 0.3 fusion.16
  36.5 0.0 copy-start.5
  36.5 0.3 fusion.9
  36.9 0.7 pad_maximum_fusion
  37.6 0.4 select_reduce_fusion
  38.0 1.3 reshape_broadcast_in_dim.4.share_ref
  39.3 0.0 copy-done.5
  39.3 0.6 reshape.185.gain_ref
  39.9 91.1 %shard_map.146 = bf16[80,2048]{1,0:T(8,128)(2,1)} custom-call(bf16[2,80,512]{2,1,0:T(8,128)(2,1)} %bitcast.47, bf16[80,2048]{1,0:T(8,128)(2,1)} %residual_ref.1, bf16[1,2048]{1,0:T(2,128)(2,1)} %reshape.185.gain_ref, f32[16,80,1]{2,1,0:T(8,128)} %reshape_broadcast_in_dim.4.share_ref, bf16[1024,2048]{1,0:T(8,128)(2,1)} %out_hbm.1, ...), custom_call_target="tpu_custom_call" | custom-call | tf_op jit(solution)/shard_map/pallas_call | solution.py:396
  131.0 1.7 %copy.39 = bf16[80,2048]{1,0:T(8,128)(2,1)} copy(bf16[80,2048]{1,0:T(8,128)(2,1)} %shard_map.146) | data formatting | bytes 655360
  (13 shorter events, 0.2 us)
Async XLA Ops:
  0.0 27.6 %copy-start = (bf16[512,512]{1,0:T(8,128)(2,1)S(1)}, bf16[512,512]{1,0:T(8,128)(2,1)}, u32[]{:S(2)}) copy-start(bf16[512,512]{1,0:T(8,128)(2,1)} %param.20) | copy-start | bytes 1572868
  27.6 1.9 %copy-start.3 = (bf16[160,512]{1,0:T(8,128)(2,1)S(1)}, bf16[160,512]{1,0:T(8,128)(2,1)}, u32[]{:S(2)}) copy-start(bf16[160,512]{1,0:T(8,128)(2,1)} %param.15) | copy-start | bytes 491524
  28.5 1.1 copy-start.1
  29.5 0.9 copy-start.4
  30.6 1.0 copy-start.6
  31.7 1.3 copy-start.2
  36.5 2.8 %copy-start.5 = (bf16[2048]{0:T(1024)(128)(2,1)S(1)}, bf16[2048]{0:T(1024)(128)(2,1)}, u32[]{:S(2)}) copy-start(bf16[2048]{0:T(1024)(128)(2,1)} %param.24) | copy-start | bytes 12292
